TPU v7x, 256 devices: a whole 4x4x8 slice. The times are simulated.
256 devices in a mesh: kv: 32 (over z, y), tp: 8 (over x, core).
Axes of the slice: x: 4, y: 4, z: 8, core: 2. Of those that a mesh axis runs over, the one named last changes fastest.
Arguments:
- stream: bfloat16 [128, 4096], P(None, ('kv', 'tp')), may hold values from -60 to 60
- memory_state: float32 [128, 32, 128, 128], P('kv', 'tp'), may hold values from -3 to 3
- attn_gain: float32 [4096], P('kv'), may hold values from 0.1 to 1.9
- query_weight: bfloat16 [4096, 4096], P('kv', 'tp'), may hold values from -0.09375 to 0.09375
- key_weight: bfloat16 [4096, 4096], P('kv', 'tp'), may hold values from -0.09375 to 0.09375
- value_weight: bfloat16 [4096, 4096], P('kv', 'tp'), may hold values from -0.09375 to 0.09375
- outgate_weight: bfloat16 [4096, 4096], P('kv', 'tp'), may hold values from -0.09375 to 0.09375
- beta_weight: bfloat16 [4096, 32], P('kv', 'tp'), may hold values from -0.09375 to 0.09375
- decay_weight: bfloat16 [4096, 32], P('kv', 'tp'), may hold values from -0.09375 to 0.09375
- decay_log: float32 [32], P('tp'), may hold values from -4 to 1
- decay_shift: float32 [32], P('tp'), may hold values from -3 to 3
- head_gain: float32 [128], replicated, may hold values from 0.1 to 1.9
- output_weight: bfloat16 [4096, 4096], P('tp', 'kv'), may hold values from -0.09375 to 0.09375
- mixer_gain: float32 [4096], P('kv'), may hold values from 0.1 to 1.9
- up_weight: bfloat16 [4096, 16384], P('kv', 'tp'), may hold values from -0.09375 to 0.09375
- down_weight: bfloat16 [16384, 4096], P('tp', 'kv'), may hold values from -0.046875 to 0.046875
Outputs:
- layer_out: bfloat16 [128, 4096], P(None, ('kv', 'tp'))
- memory_next: float32 [128, 32, 128, 128], P('kv', 'tp')
All inputs are finite; a program needn't handle non-finite values.
Results may differ from a plain program's by a relative error of at most 0.025.
Values may be sent and summed in bfloat16 or wider, within the bound.
A program may use at most 64 MiB of HBM per device.

v0:
```python
import jax
import jax.numpy as jnp
from jax import lax
from jax.sharding import PartitionSpec as P

D = 4096
HEAD_DIM = 128
epsilon = 1e-06


def split_up(value, dim, length):
    dims = value.shape
    pieces = value.reshape(*dims[:dim], length, dims[dim] // length, *dims[dim + 1 :])
    return jnp.moveaxis(pieces, dim, 0)


def sent_and_summed(value, axis, dim):
    length = lax.axis_size(axis)
    pieces = lax.all_to_all(split_up(value, dim, length), axis, 0, 0, tiled=True)
    return jnp.sum(pieces.astype(jnp.float32), axis=0)


def side_by_side(arrays, axis, dim, along):
    columns = [a.reshape(*a.shape[:along], -1) for a in arrays]
    both = jnp.concatenate(columns, axis=along)
    out, at, gathered = (sent_and_summed(both, axis, dim), 0, [])
    for a, column in zip(arrays, columns):
        share = out[..., at : at + column.shape[along]]
        gathered.append(share.reshape(*share.shape[:along], *a.shape[along:]))
        at += column.shape[along]
    return tuple(gathered)


def joined_along(pieces, dim):
    dims = list(pieces.shape[1:])
    dims[dim] *= pieces.shape[0]
    return jnp.moveaxis(pieces, 0, dim).reshape(dims)


def copy_for_each(value, axis):
    copies = jnp.broadcast_to(value, (lax.axis_size(axis), *value.shape))
    return lax.all_to_all(copies, axis, split_axis=0, concat_axis=0, tiled=True)


def collect(value, axis, dim):
    return joined_along(copy_for_each(value, axis), dim)


def sent_and_summed_2(value, axis, dim):
    pieces = split_up(value, dim, lax.axis_size(axis))
    arrived = lax.all_to_all(pieces, axis, split_axis=0, concat_axis=0, tiled=True)
    return arrived.sum(axis=0)


def gathered_rows(stream, gain_vec):
    gathered = lax.all_gather(stream, "tp", axis=1, tiled=True)
    widened = gathered.astype(jnp.float32)
    squares = jnp.sum(widened * widened, axis=1)
    scaled = (widened * gain_vec).astype(jnp.bfloat16)
    return (scaled, squares)


def unit_rows(values):
    return values * lax.rsqrt(jnp.sum(values * values, axis=-1, keepdims=True) + epsilon)


def head_output(
    memory_state,
    query_sum,
    key_sum,
    value_sum,
    gate_sum,
    beta_sum,
    decay_sum,
    decay_log,
    decay_shift,
    head_gain,
):
    row_count = query_sum.shape[0]
    head_count = beta_sum.shape[1]

    def to_heads(values):
        return values.reshape(row_count, head_count, HEAD_DIM)

    query_heads = unit_rows(jax.nn.silu(to_heads(query_sum))) * HEAD_DIM ** (-0.5)
    key_heads = unit_rows(jax.nn.silu(to_heads(key_sum)))
    value_heads = jax.nn.silu(to_heads(value_sum))
    beta_heads = jax.nn.sigmoid(beta_sum)
    decay_heads = jnp.exp(-jnp.exp(decay_log) * jax.nn.softplus(decay_sum + decay_shift))
    kept_state = memory_state * decay_heads[:, :, None, None]
    recalled = jnp.einsum("bhkv,bhk->bhv", kept_state, key_heads)
    correction = beta_heads[:, :, None] * (value_heads - recalled)
    memory_next = kept_state + key_heads[:, :, :, None] * correction[:, :, None, :]
    readout = jnp.einsum("bhkv,bhk->bhv", memory_next, query_heads)
    normed = readout * lax.rsqrt(jnp.mean(readout * readout, axis=-1, keepdims=True) + epsilon)
    gated = normed * head_gain * jax.nn.silu(to_heads(gate_sum))
    return (gated.reshape(row_count, head_count * HEAD_DIM).astype(jnp.bfloat16), memory_next)


def shards(
    stream,
    memory_state,
    attn_gain,
    query_weight,
    key_weight,
    value_weight,
    outgate_weight,
    beta_weight,
    decay_weight,
    decay_log,
    decay_shift,
    head_gain,
    output_weight,
    mixer_gain,
    up_weight,
    down_weight,
):
    scaled, squares = gathered_rows(stream, attn_gain)

    def product(weight):
        return jnp.dot(scaled, weight, preferred_element_type=jnp.float32)

    query_sum, key_sum, value_sum, gate_sum, beta_sum, decay_sum, own_squares = side_by_side(
        (
            product(query_weight).astype(jnp.bfloat16),
            product(key_weight).astype(jnp.bfloat16),
            product(value_weight).astype(jnp.bfloat16),
            product(outgate_weight).astype(jnp.bfloat16),
            product(beta_weight).astype(jnp.bfloat16),
            product(decay_weight).astype(jnp.bfloat16),
            squares.astype(jnp.bfloat16),
        ),
        "kv",
        0,
        1,
    )
    factor = lax.rsqrt(own_squares / D + epsilon)[:, None]
    heads_out, memory_next = head_output(
        memory_state,
        query_sum * factor,
        key_sum * factor,
        value_sum * factor,
        gate_sum * factor,
        beta_sum * factor,
        decay_sum * factor,
        decay_log,
        decay_shift,
        head_gain,
    )
    attn_rows = jnp.dot(
        collect(heads_out, "kv", 0), output_weight, preferred_element_type=jnp.float32
    )
    attn_mine = sent_and_summed_2(attn_rows, "tp", 1)
    middle = (stream.astype(jnp.float32) + attn_mine).astype(jnp.bfloat16)
    scaled_mix, squares_mix = gathered_rows(middle, mixer_gain)
    up_part = jnp.dot(scaled_mix, up_weight, preferred_element_type=jnp.float32)
    up_mine, square_mine = side_by_side(
        (up_part.astype(jnp.bfloat16), squares_mix.astype(jnp.bfloat16)), "kv", 0, 1
    )
    hidden = jnp.square(
        jax.nn.relu(up_mine * lax.rsqrt(square_mine / D + epsilon)[:, None])
    ).astype(jnp.bfloat16)
    down_rows = jnp.dot(collect(hidden, "kv", 0), down_weight, preferred_element_type=jnp.float32)
    mixer_mine = lax.psum_scatter(
        down_rows.astype(jnp.bfloat16), "tp", scatter_dimension=1, tiled=True
    ).astype(jnp.float32)
    layer_out = (middle.astype(jnp.float32) + mixer_mine).astype(jnp.bfloat16)
    return (layer_out, memory_next)


def solution(mesh):
    in_specs = (
        P(None, ("kv", "tp")),
        P("kv", "tp", None, None),
        P("kv"),
        P("kv", "tp"),
        P("kv", "tp"),
        P("kv", "tp"),
        P("kv", "tp"),
        P("kv", "tp"),
        P("kv", "tp"),
        P("tp"),
        P("tp"),
        P(),
        P("tp", "kv"),
        P("kv"),
        P("kv", "tp"),
        P("tp", "kv"),
    )
    out_specs = (P(None, ("kv", "tp")), P("kv", "tp", None, None))
    return jax.shard_map(shards, mesh=mesh, in_specs=in_specs, out_specs=out_specs, check_vma=False)
```

profile of v0, /device:TPU:8, one launch (start us, length us, event | category | flops | bytes accessed | tf_op | source)
XLA Modules:
  0.0 182.4 jit_solution(9769738742397507875)
XLA Ops:
  7.2 13.5 %all_gather.6 = bf16[128,128]{0,1:T(8,128)(2,1)S(1)} all-gather(bf16[128,16]{0,1:T(8,128)(2,1)} %param.16), channel_id=1, replica_groups=mesh['kv'=32,'tp'=8] {'tp'}, dimensions={1}, use_global_device_ids=true | all-gather | bytes 36864 | tf_op jit(solution)/shard_map/all_gather | solution.py:56
  20.8 0.9 convolution_convert_fusion.7
  21.7 0.9 convolution_convert_fusion.6
  23.1 1.2 convolution_convert_fusion.3
  24.3 1.2 convolution_convert_fusion.2
  25.9 0.3 convolution_convert_fusion.4
  26.3 2.0 %concatenate.28 = bf16[32,4,2057]{2,1,0:T(4,128)(2,1)} concatenate(bf16[32,4,512]{2,1,0:T(4,128)(2,1)S(1)} %concatenate.22, bf16[32,4,512]{2,1,0:T(4,128)(2,1)S(1)} %concatenate.23, bf16[32,4,512]{2,1,0:T(4,128)(2,1)S(1)} %concatenate.24, bf16[32,4,512]{2,1,0:T(4,128)(2,1)S(1)} %concatenate.25, bf16[32,4,4]{2,1,0:T(4,128)(2,1)S(1)} %bitcast.38, bf16[32,4,4]{2,1,0:T(4,128)(2,1)S(1)} %bitcast.37, ...), dimensions={2} | concatenate | bytes 1053184 | tf_op jit(solution)/shard_map/concatenate | solution.py:25
  28.3 11.8 %all-to-all-start = ((bf16[32,4,2057]{2,1,0:T(4,128)(2,1)}), bf16[32,4,2057]{2,1,0:T(4,128)(2,1)S(1)}, u32[]{:S(2)}, u32[]{:S(2)}) async-start(bf16[32,4,2057]{2,1,0:T(4,128)(2,1)} %concatenate.28), calls=%async_computation | async-start | bytes 1114112 | tf_op jit(solution)/shard_map/all_to_all | solution.py:19
  40.2 18.0 %all-to-all-done = bf16[32,4,2057]{2,1,0:T(4,128)(2,1)S(1)} async-done(((bf16[32,4,2057]{2,1,0:T(4,128)(2,1)}), bf16[32,4,2057]{2,1,0:T(4,128)(2,1)S(1)}, u32[]{:S(2)}, u32[]{:S(2)}) %all-to-all-start) | async-done | bytes 526624 | tf_op jit(solution)/shard_map/all_to_all | solution.py:19
  59.3 0.3 fusion
  59.6 0.4 multiply_add_fusion
  60.4 0.3 copy-done.11
  60.8 0.7 broadcast_in_dim.4
  61.5 5.6 %all-to-all-start.1 = ((bf16[32,4,512]{2,1,0:T(4,128)(2,1)}), bf16[32,4,512]{2,1,0:T(4,128)(2,1)S(1)}, u32[]{:S(2)}, u32[]{:S(2)}) async-start(bf16[32,4,512]{2,1,0:T(4,128)(2,1)} %broadcast_in_dim.4), calls=%async_computation.1 | async-start | bytes 262144 | tf_op jit(solution)/shard_map/all_to_all | solution.py:42
  67.3 8.6 %all-to-all-done.1 = bf16[32,4,512]{2,1,0:T(4,128)(2,1)S(1)} async-done(((bf16[32,4,512]{2,1,0:T(4,128)(2,1)}), bf16[32,4,512]{2,1,0:T(4,128)(2,1)S(1)}, u32[]{:S(2)}, u32[]{:S(2)}) %all-to-all-start.1) | async-done | bytes 131104 | tf_op jit(solution)/shard_map/all_to_all | solution.py:42
  76.1 9.1 %all_to_all.25 = f32[8,128,16]{1,2,0:T(8,128)S(1)} all-to-all(f32[8,128,16]{1,2,0:T(8,128)S(1)} %convolution_bitcast_fusion), channel_id=1, replica_groups=mesh['kv'=32,'tp'=8] {'tp'}, dimensions={0} | all-to-all | bytes 131072 | tf_op jit(solution)/shard_map/all_to_all | solution.py:51
  85.2 12.9 %all_gather.7 = bf16[128,128]{0,1:T(8,128)(2,1)S(1)} all-gather(bf16[128,16]{0,1:T(8,128)(2,1)S(1)} %add_convert_fusion.1), channel_id=1, replica_groups=mesh['kv'=32,'tp'=8] {'tp'}, dimensions={1}, use_global_device_ids=true | all-gather | bytes 36864 | tf_op jit(solution)/shard_map/all_gather | solution.py:56
  98.4 0.4 convolution_convert_fusion
  99.0 0.3 pad_maximum_fusion
  99.3 23.0 %all_to_all.26 = bf16[32,4,2049]{2,1,0:T(4,128)(2,1)S(1)} all-to-all(bf16[32,4,2049]{2,1,0:T(4,128)(2,1)S(1)} %pad_maximum_fusion), channel_id=1, replica_groups=mesh['kv'=32,'tp'=8] {'kv'}, dimensions={0} | all-to-all | bytes 1049088 | tf_op jit(solution)/shard_map/all_to_all | solution.py:19
  123.0 21.7 %all_to_all.27 = bf16[32,4,2048]{2,1,0:T(4,128)(2,1)S(1)} all-to-all(bf16[32,4,2048]{2,1,0:T(4,128)(2,1)S(1)} %broadcast_in_dim.5), channel_id=1, replica_groups=mesh['kv'=32,'tp'=8] {'kv'}, dimensions={0} | all-to-all | bytes 1048576 | tf_op jit(solution)/shard_map/all_to_all | solution.py:42
  144.9 0.9 convolution_convert_fusion.5
  145.8 28.5 %reduce-scatter.2.cloned.1.call-done = bf16[128,16]{0,1:T(8,128)(2,1)} async-done(((bf16[128,128]{0,1:T(8,128)(2,1)}), bf16[128,16]{0,1:T(8,128)(2,1)}) %reduce-scatter.2.cloned.1.call-update) | async-done | bytes 4112 | tf_op jit(solution)/shard_map/reduce_scatter | solution.py:164
  174.3 1.3 add_convert_fusion
  (70 shorter events, 4.2 us)
Async XLA Ops:
  7.2 91.3 %copy-start = (bf16[128,2048]{1,0:T(8,128)(2,1)S(1)}, bf16[128,2048]{1,0:T(8,128)(2,1)}, u32[]{:S(2)}) copy-start(bf16[128,2048]{1,0:T(8,128)(2,1)} %param.30) | copy-start | bytes 1572868
  7.2 18.4 %copy-start.8 = (f32[128]{0:T(128)S(1)}, f32[128]{0:T(128)}, u32[]{:S(2)}) copy-start(f32[128]{0:T(128)} %param.18) | copy-start | bytes 1540
  7.2 18.4 %copy-start.4 = (bf16[128,512]{1,0:T(8,128)(2,1)S(1)}, bf16[128,512]{1,0:T(8,128)(2,1)}, u32[]{:S(2)}) copy-start(bf16[128,512]{1,0:T(8,128)(2,1)} %param.22) | copy-start | bytes 393220
  7.2 18.7 %copy-start.5 = (bf16[128,512]{1,0:T(8,128)(2,1)S(1)}, bf16[128,512]{1,0:T(8,128)(2,1)}, u32[]{:S(2)}) copy-start(bf16[128,512]{1,0:T(8,128)(2,1)} %param.19) | copy-start | bytes 393220
  26.3 13.9 %copy-start.12 = (f32[4]{0:T(128)S(1)}, f32[4]{0:T(128)}, u32[]{:S(2)}) copy-start(f32[4]{0:T(128)} %param.25) | copy-start | bytes 52
  28.3 30.8 %copy-start.10 = (f32[4]{0:T(128)S(1)}, f32[4]{0:T(128)}, u32[]{:S(2)}) copy-start(f32[4]{0:T(128)} %param.26) | copy-start | bytes 52
  28.3 30.9 %copy-start.1 = (f32[4,4,128,128]{3,2,1,0:T(8,128)S(1)}, f32[4,4,128,128]{3,2,1,0:T(8,128)}, u32[]{:S(2)}) copy-start(f32[4,4,128,128]{3,2,1,0:T(8,128)} %param.17) | copy-start | bytes 3145732
  28.3 29.9 %all-to-all-start = ((bf16[32,4,2057]{2,1,0:T(4,128)(2,1)}), bf16[32,4,2057]{2,1,0:T(4,128)(2,1)S(1)}, u32[]{:S(2)}, u32[]{:S(2)}) async-start(bf16[32,4,2057]{2,1,0:T(4,128)(2,1)} %concatenate.28), calls=%async_computation | async-start | bytes 1114112 | tf_op jit(solution)/shard_map/all_to_all | solution.py:19
  60.0 16.1 %copy-start.2 = (f32[4,4,128,128]{3,2,1,0:T(8,128)}, f32[4,4,128,128]{3,2,1,0:T(8,128)S(1)}, u32[]{:S(2)}) copy-start(f32[4,4,128,128]{3,2,1,0:T(8,128)S(1)} %multiply_add_fusion) | copy-start | bytes 3145732
  60.1 0.7 copy-start.11
  60.1 7.1 %copy-start.6 = (bf16[512,128]{1,0:T(8,128)(2,1)S(1)}, bf16[512,128]{1,0:T(8,128)(2,1)}, u32[]{:S(2)}) copy-start(bf16[512,128]{1,0:T(8,128)(2,1)} %param.28) | copy-start | bytes 393220
  60.1 25.1 %copy-start.7 = (bf16[128,16]{0,1:T(8,128)(2,1)S(1)}, bf16[128,16]{0,1:T(8,128)(2,1)}, u32[]{:S(2)}) copy-start(bf16[128,16]{0,1:T(8,128)(2,1)} %param.16) | copy-start | bytes 12292
  60.3 38.1 %copy-start.9 = (f32[128]{0:T(128)S(1)}, f32[128]{0:T(128)}, u32[]{:S(2)}) copy-start(f32[128]{0:T(128)} %param.29) | copy-start | bytes 1540
  61.5 14.4 %all-to-all-start.1 = ((bf16[32,4,512]{2,1,0:T(4,128)(2,1)}), bf16[32,4,512]{2,1,0:T(4,128)(2,1)S(1)}, u32[]{:S(2)}, u32[]{:S(2)}) async-start(bf16[32,4,512]{2,1,0:T(4,128)(2,1)} %broadcast_in_dim.4), calls=%async_computation.1 | async-start | bytes 262144 | tf_op jit(solution)/shard_map/all_to_all | solution.py:42
  67.1 107.2 %reduce-scatter.2.cloned.1.call-start = ((), (), s32[]{:S(2)}) async-start(), calls=%async_computation.6 | async-start | bytes 36864 | tf_op jit(solution)/shard_map/reduce_scatter | solution.py:164
  123.0 21.8 %copy-start.3 = (bf16[2048,128]{1,0:T(8,128)(2,1)S(1)}, bf16[2048,128]{1,0:T(8,128)(2,1)}, u32[]{:S(2)}) copy-start(bf16[2048,128]{1,0:T(8,128)(2,1)} %param.31) | copy-start | bytes 1572868
Sparse Core Ops, SparseCore 0:
  145.9 28.2 reduce-scatter.1
where the time goes:
time: 183 us; the launch traced here: 182 us
  blocking collectives  80.2 us (44%)
  waiting for transfers between devices  55.1 us (30%)
  starting transfers between devices  17.4 us (10%)
  between operations  14.4 us (8%)
  matrix products  6.8 us (4%)
  local copies, waits for them, and re-layouts  4.73 us (3%)
  other arithmetic  3.69 us (2%)
    reduce_scatter x1, waiting for transfers between devices, shards(): lax.psum_scatter(down_rows.astype(jnp.bfloat16), 'tp', scatter_dimension=...  28.5 us
    all_gather x2, blocking collectives, gathered_rows(): gathered = lax.all_gather(stream, 'tp', axis=1, tiled=True)  26.4 us
    all_to_all x1, blocking collectives, sent_and_summed(): lax.all_to_all(split_up(value, dim, length), axis, 0, 0, tiled=True)  23 us
    all_to_all x1, blocking collectives, copy_for_each(): return lax.all_to_all(copies, axis, split_axis=0, concat_axis=0, tiled=True)  21.7 us
    all_to_all x1, waiting for transfers between devices, sent_and_summed(): lax.all_to_all(split_up(value, dim, length), axis, 0, 0, tiled=True)  18 us
    all_to_all x1, starting transfers between devices, sent_and_summed(): lax.all_to_all(split_up(value, dim, length), axis, 0, 0, tiled=True)  11.8 us
    all_to_all x1, blocking collectives, sent_and_summed_2(): lax.all_to_all(pieces, axis, split_axis=0, concat_axis=0, tiled=True)  9.07 us
    all_to_all x1, waiting for transfers between devices, copy_for_each(): return lax.all_to_all(copies, axis, split_axis=0, concat_axis=0, tiled=True)  8.64 us
  transfers between devices with their start and end apart: 3, of which 3 were waited for; matrix products, arithmetic and copies ran while one was open for 0% of the time, Pallas kernels for 0%

commit v1 on v0

--- a/solution.py
+++ b/solution.py
@@ -6,6 +6,14 @@
 D = 4096
 HEAD_DIM = 128
 epsilon = 1e-06
+
+
+def gather_from_all(shard, axis, dim):
+    peers = lax.axis_size(axis)
+    repeats = [peers if d == dim else 1 for d in range(shard.ndim)]
+    return lax.all_to_all(
+        jnp.tile(shard, repeats), axis, split_axis=dim, concat_axis=dim, tiled=True
+    )
 
 
 def split_up(value, dim, length):
@@ -53,7 +61,7 @@
 
 
 def gathered_rows(stream, gain_vec):
-    gathered = lax.all_gather(stream, "tp", axis=1, tiled=True)
+    gathered = gather_from_all(stream, "tp", 1)
     widened = gathered.astype(jnp.float32)
     squares = jnp.sum(widened * widened, axis=1)
     scaled = (widened * gain_vec).astype(jnp.bfloat16)

time: 183 us -> 172 us (0.940)
  blocking collectives: 80.2 us -> 69.1 us
    all_gather x2 -> x0, blocking collectives: 26.4 us -> none  [gathered_rows(): gathered = lax.all_gather(stream, 'tp', axis=1, tiled=True)]
    all_to_all x0 -> x2, blocking collectives: none -> 17.3 us  [gather_from_all(): lax.all_to_all(jnp.tile(shard, repeats), axis, split_axis=dim, concat_axi...]
where the time goes in v1:
time: 172 us
  blocking collectives  69.1 us (40%)
  waiting for transfers between devices  54.4 us (32%)
  starting transfers between devices  17.4 us (10%)
  between operations  14.4 us (8%)
  matrix products  6.26 us (4%)
  local copies, waits for them, and re-layouts  5.49 us (3%)
  other arithmetic  4.51 us (3%)
    reduce_scatter x1, waiting for transfers between devices, shards(): lax.psum_scatter(down_rows.astype(jnp.bfloat16), 'tp', scatter_dimension=...  28.2 us
    all_to_all x1, blocking collectives, sent_and_summed(): lax.all_to_all(split_up(value, dim, length), axis, 0, 0, tiled=True)  22.4 us
    all_to_all x1, blocking collectives, copy_for_each(): return lax.all_to_all(copies, axis, split_axis=0, concat_axis=0, tiled=True)  21.4 us
    all_to_all x1, waiting for transfers between devices, sent_and_summed(): lax.all_to_all(split_up(value, dim, length), axis, 0, 0, tiled=True)  17.4 us
    all_to_all x2, blocking collectives, gather_from_all(): lax.all_to_all(jnp.tile(shard, repeats), axis, split_axis=dim, concat_axi...  17.3 us
    all_to_all x1, starting transfers between devices, sent_and_summed(): lax.all_to_all(split_up(value, dim, length), axis, 0, 0, tiled=True)  11.8 us
    all_to_all x1, waiting for transfers between devices, copy_for_each(): return lax.all_to_all(copies, axis, split_axis=0, concat_axis=0, tiled=True)  8.73 us
    all_to_all x1, blocking collectives, sent_and_summed_2(): lax.all_to_all(pieces, axis, split_axis=0, concat_axis=0, tiled=True)  8 us
  transfers between devices with their start and end apart: 3, of which 3 were waited for; matrix products, arithmetic and copies ran while one was open for 0% of the time, Pallas kernels for 0%

profile of v1, /device:TPU:8, one launch (start us, length us, event | category | flops | bytes accessed | tf_op | source)
XLA Modules:
  0.0 171.6 jit_solution(4297507108065409718)
XLA Ops:
  7.2 0.8 tile.4
  8.0 9.5 %all_to_all.37 = bf16[128,8,16]{0,2,1:T(8,128)(2,1)S(1)} all-to-all(bf16[128,8,16]{0,2,1:T(8,128)(2,1)S(1)} %tile.4), channel_id=1, replica_groups=mesh['kv'=32,'tp'=8] {'tp'}, dimensions={1} | all-to-all | bytes 65536 | tf_op jit(solution)/shard_map/all_to_all | solution.py:14
  17.5 0.7 fusion.4
  18.2 0.8 convolution_convert_fusion.6
  19.0 0.8 convolution_convert_fusion.7
  20.4 1.1 convolution_convert_fusion.1
  21.6 1.1 convolution_convert_fusion.2
  23.3 2.0 %concatenate.28 = bf16[32,4,2057]{2,1,0:T(4,128)(2,1)} concatenate(bf16[32,4,512]{2,1,0:T(4,128)(2,1)S(1)} %concatenate.22, bf16[32,4,512]{2,1,0:T(4,128)(2,1)S(1)} %concatenate.23, bf16[32,4,512]{2,1,0:T(4,128)(2,1)S(1)} %concatenate.24, bf16[32,4,512]{2,1,0:T(4,128)(2,1)S(1)} %concatenate.25, bf16[32,4,4]{2,1,0:T(4,128)(2,1)S(1)} %bitcast.52, bf16[32,4,4]{2,1,0:T(4,128)(2,1)S(1)} %bitcast.53, ...), dimensions={2} | concatenate | bytes 1053184 | tf_op jit(solution)/shard_map/concatenate | solution.py:33
  25.3 11.8 %all-to-all-start.1 = ((bf16[32,4,2057]{2,1,0:T(4,128)(2,1)}), bf16[32,4,2057]{2,1,0:T(4,128)(2,1)S(1)}, u32[]{:S(2)}, u32[]{:S(2)}) async-start(bf16[32,4,2057]{2,1,0:T(4,128)(2,1)} %concatenate.28), calls=%async_computation.1 | async-start | bytes 1114112 | tf_op jit(solution)/shard_map/all_to_all | solution.py:27
  37.2 17.4 %all-to-all-done.1 = bf16[32,4,2057]{2,1,0:T(4,128)(2,1)S(1)} async-done(((bf16[32,4,2057]{2,1,0:T(4,128)(2,1)}), bf16[32,4,2057]{2,1,0:T(4,128)(2,1)S(1)}, u32[]{:S(2)}, u32[]{:S(2)}) %all-to-all-start.1) | async-done | bytes 526624 | tf_op jit(solution)/shard_map/all_to_all | solution.py:27
  55.7 0.3 fusion
  56.1 0.4 multiply_add_fusion
  56.9 0.3 copy-done.10
  57.2 0.7 broadcast_in_dim.4
  57.9 5.6 %all-to-all-start.2 = ((bf16[32,4,512]{2,1,0:T(4,128)(2,1)}), bf16[32,4,512]{2,1,0:T(4,128)(2,1)S(1)}, u32[]{:S(2)}, u32[]{:S(2)}) async-start(bf16[32,4,512]{2,1,0:T(4,128)(2,1)} %broadcast_in_dim.4), calls=%async_computation.2 | async-start | bytes 262144 | tf_op jit(solution)/shard_map/all_to_all | solution.py:50
  63.7 8.7 %all-to-all-done.2 = bf16[32,4,512]{2,1,0:T(4,128)(2,1)S(1)} async-done(((bf16[32,4,512]{2,1,0:T(4,128)(2,1)}), bf16[32,4,512]{2,1,0:T(4,128)(2,1)S(1)}, u32[]{:S(2)}, u32[]{:S(2)}) %all-to-all-start.2) | async-done | bytes 131104 | tf_op jit(solution)/shard_map/all_to_all | solution.py:50
  72.7 8.0 %all_to_all.38 = f32[8,128,16]{1,2,0:T(8,128)S(1)} all-to-all(f32[8,128,16]{1,2,0:T(8,128)S(1)} %convolution_bitcast_fusion), channel_id=1, replica_groups=mesh['kv'=32,'tp'=8] {'tp'}, dimensions={0} | all-to-all | bytes 131072 | tf_op jit(solution)/shard_map/all_to_all | solution.py:59
  80.7 7.8 %all_to_all.39 = bf16[128,8,16]{0,2,1:T(8,128)(2,1)S(1)} all-to-all(bf16[128,8,16]{0,2,1:T(8,128)(2,1)S(1)} %tile.5), channel_id=1, replica_groups=mesh['kv'=32,'tp'=8] {'tp'}, dimensions={1} | all-to-all | bytes 65536 | tf_op jit(solution)/shard_map/all_to_all | solution.py:14
  88.9 0.3 convolution_convert_fusion
  89.7 22.4 %all_to_all.40 = bf16[32,4,2049]{2,1,0:T(4,128)(2,1)S(1)} all-to-all(bf16[32,4,2049]{2,1,0:T(4,128)(2,1)S(1)} %pad_maximum_fusion), channel_id=1, replica_groups=mesh['kv'=32,'tp'=8] {'kv'}, dimensions={0} | all-to-all | bytes 1049088 | tf_op jit(solution)/shard_map/all_to_all | solution.py:27
  112.8 21.4 %all_to_all.41 = bf16[32,4,2048]{2,1,0:T(4,128)(2,1)S(1)} all-to-all(bf16[32,4,2048]{2,1,0:T(4,128)(2,1)S(1)} %broadcast_in_dim.5), channel_id=1, replica_groups=mesh['kv'=32,'tp'=8] {'kv'}, dimensions={0} | all-to-all | bytes 1048576 | tf_op jit(solution)/shard_map/all_to_all | solution.py:50
  134.3 0.9 convolution_convert_fusion.5
  135.3 28.2 %reduce-scatter.2.cloned.1.call-done = bf16[128,16]{0,1:T(8,128)(2,1)} async-done(((bf16[128,128]{0,1:T(8,128)(2,1)}), bf16[128,16]{0,1:T(8,128)(2,1)}) %reduce-scatter.2.cloned.1.call-update) | async-done | bytes 4112 | tf_op jit(solution)/shard_map/reduce_scatter | solution.py:172
  163.5 1.3 add_convert_fusion
  (72 shorter events, 4.7 us)
Async XLA Ops:
  7.2 81.7 %copy-start = (bf16[128,2048]{1,0:T(8,128)(2,1)S(1)}, bf16[128,2048]{1,0:T(8,128)(2,1)}, u32[]{:S(2)}) copy-start(bf16[128,2048]{1,0:T(8,128)(2,1)} %param.30) | copy-start | bytes 1572868
  7.2 15.6 %copy-start.4 = (bf16[128,512]{1,0:T(8,128)(2,1)S(1)}, bf16[128,512]{1,0:T(8,128)(2,1)}, u32[]{:S(2)}) copy-start(bf16[128,512]{1,0:T(8,128)(2,1)} %param.20) | copy-start | bytes 393220
  7.2 15.8 %copy-start.5 = (bf16[128,512]{1,0:T(8,128)(2,1)S(1)}, bf16[128,512]{1,0:T(8,128)(2,1)}, u32[]{:S(2)}) copy-start(bf16[128,512]{1,0:T(8,128)(2,1)} %param.19) | copy-start | bytes 393220
  23.3 13.9 %copy-start.11 = (f32[4]{0:T(128)S(1)}, f32[4]{0:T(128)}, u32[]{:S(2)}) copy-start(f32[4]{0:T(128)} %param.25) | copy-start | bytes 52
  25.3 30.3 %copy-start.9 = (f32[4]{0:T(128)S(1)}, f32[4]{0:T(128)}, u32[]{:S(2)}) copy-start(f32[4]{0:T(128)} %param.26) | copy-start | bytes 52
  25.3 30.4 %copy-start.1 = (f32[4,4,128,128]{3,2,1,0:T(8,128)S(1)}, f32[4,4,128,128]{3,2,1,0:T(8,128)}, u32[]{:S(2)}) copy-start(f32[4,4,128,128]{3,2,1,0:T(8,128)} %param.17) | copy-start | bytes 3145732
  25.3 29.3 %all-to-all-start.1 = ((bf16[32,4,2057]{2,1,0:T(4,128)(2,1)}), bf16[32,4,2057]{2,1,0:T(4,128)(2,1)S(1)}, u32[]{:S(2)}, u32[]{:S(2)}) async-start(bf16[32,4,2057]{2,1,0:T(4,128)(2,1)} %concatenate.28), calls=%async_computation.1 | async-start | bytes 1114112 | tf_op jit(solution)/shard_map/all_to_all | solution.py:27
  56.5 16.2 %copy-start.2 = (f32[4,4,128,128]{3,2,1,0:T(8,128)}, f32[4,4,128,128]{3,2,1,0:T(8,128)S(1)}, u32[]{:S(2)}) copy-start(f32[4,4,128,128]{3,2,1,0:T(8,128)S(1)} %multiply_add_fusion) | copy-start | bytes 3145732
  56.5 0.7 copy-start.10
  56.5 7.1 %copy-start.6 = (bf16[512,128]{1,0:T(8,128)(2,1)S(1)}, bf16[512,128]{1,0:T(8,128)(2,1)}, u32[]{:S(2)}) copy-start(bf16[512,128]{1,0:T(8,128)(2,1)} %param.28) | copy-start | bytes 393220
  56.5 24.2 %copy-start.7 = (bf16[128,16]{0,1:T(8,128)(2,1)S(1)}, bf16[128,16]{0,1:T(8,128)(2,1)}, u32[]{:S(2)}) copy-start(bf16[128,16]{0,1:T(8,128)(2,1)} %param.16) | copy-start | bytes 12292
  56.8 32.0 %copy-start.8 = (f32[128]{0:T(128)S(1)}, f32[128]{0:T(128)}, u32[]{:S(2)}) copy-start(f32[128]{0:T(128)} %param.29) | copy-start | bytes 1540
  57.9 14.5 %all-to-all-start.2 = ((bf16[32,4,512]{2,1,0:T(4,128)(2,1)}), bf16[32,4,512]{2,1,0:T(4,128)(2,1)S(1)}, u32[]{:S(2)}, u32[]{:S(2)}) async-start(bf16[32,4,512]{2,1,0:T(4,128)(2,1)} %broadcast_in_dim.4), calls=%async_computation.2 | async-start | bytes 262144 | tf_op jit(solution)/shard_map/all_to_all | solution.py:50
  63.5 100.0 %reduce-scatter.2.cloned.1.call-start = ((), (), s32[]{:S(2)}) async-start(), calls=%async_computation.8 | async-start | bytes 36864 | tf_op jit(solution)/shard_map/reduce_scatter | solution.py:172
  112.8 21.5 %copy-start.3 = (bf16[2048,128]{1,0:T(8,128)(2,1)S(1)}, bf16[2048,128]{1,0:T(8,128)(2,1)}, u32[]{:S(2)}) copy-start(bf16[2048,128]{1,0:T(8,128)(2,1)} %param.31) | copy-start | bytes 1572868
Sparse Core Ops, SparseCore 0:
  135.4 28.0 reduce-scatter.1
